TPU v7x, 32 devices: a whole 2x2x4 slice. The times are simulated.
32 devices in a mesh: sp: 4 (over z), fs: 4 (over y, x), tp: 2 (over core).
Axes of the slice: x: 2, y: 2, z: 4, core: 2. Of those that a mesh axis runs over, the one named last changes fastest.
Arguments:
- tokens: bfloat16 [4, 1024, 2048], P('fs', 'sp', 'tp'), may hold values from -6 to 6
- norm_gain: float32 [2048], replicated, may hold values from 0.1 to 1.9
- memory_query: bfloat16 [2048, 1024], P('fs', 'tp'), may hold values from -0.125 to 0.125
- memory_key: bfloat16 [2048, 1024], P('fs', 'tp'), may hold values from -0.125 to 0.125
- memory_value: bfloat16 [2048, 1024], P('fs', 'tp'), may hold values from -0.125 to 0.125
- memory_outgate: bfloat16 [2048, 1024], P('fs', 'tp'), may hold values from -0.125 to 0.125
- memory_ingate: bfloat16 [2048, 4], P(None, 'tp'), may hold values from -0.125 to 0.125
- memory_forget: bfloat16 [2048, 4], P(None, 'tp'), may hold values from -0.125 to 0.125
- forget_bias: float32 [4], P('tp'), may hold values from 3 to 13
- forget_shift: float32 [4, 1024, 4], P('fs', 'sp', 'tp'), may hold values from -1.6 to 0
- stick_query: bfloat16 [2048, 512], P(None, 'tp'), may hold values from -0.125 to 0.125
- stick_key: bfloat16 [2048, 512], P(None, 'tp'), may hold values from -0.125 to 0.125
- stick_value: bfloat16 [2048, 512], P(None, 'tp'), may hold values from -0.125 to 0.125
- stick_bias: float32 [4], P('tp'), may hold values from -11 to -2
- memory_gain: float32 [1024], P('tp'), may hold values from 0.1 to 1.9
- stick_gain: float32 [512], P('tp'), may hold values from 0.1 to 1.9
- out_memory: bfloat16 [1024, 2048], P('tp'), may hold values from -0.15625 to 0.15625
- out_stick: bfloat16 [512, 2048], P('tp'), may hold values from -0.15625 to 0.15625
Outputs:
- mixed: bfloat16 [4, 1024, 2048], P('fs', ('sp', 'tp'))
All inputs are finite; a program needn't handle non-finite values.
Results may differ from a plain program's by a relative error of at most 0.015.
Values may be sent and summed in bfloat16 or wider, within the bound.
A program may use at most 128 MiB of HBM per device.

v0:
```python
import jax
import jax.numpy as jnp
from jax import lax
from jax.sharding import PartitionSpec as P

BLOCK = 128


epsilon = 1e-06
floor_neg = -1e30
peak_value = lax.Precision.HIGHEST


def carried_in(array, axis, join, neutral):
    place = lax.axis_index(axis)
    gathered = jax.tree.map(
        lambda a, kind: lax.all_gather(a.astype(kind), axis),
        array,
        (jnp.bfloat16, jnp.bfloat16, jnp.bfloat16),
    )
    state = jax.tree.map(lambda a, e: jnp.zeros_like(a) + jnp.asarray(e, a.dtype), array, neutral)

    def one(turn, state):
        return join(
            state,
            jax.tree.map(
                lambda a, own: lax.dynamic_index_in_dim(a, turn, 0, False).astype(own.dtype),
                gathered,
                array,
            ),
        )

    return lax.fori_loop(0, place, one, state)


def shifted(block, axis, distance):
    devices = range(lax.axis_size(axis))
    route = [(i - distance, i) for i in devices if i - distance in devices]
    return lax.ppermute(block, axis, route)


def rounded(values):
    return lax.optimization_barrier(values.astype(jnp.bfloat16)).astype(jnp.float32)


def per_head_norm(values, gain):
    scale = lax.rsqrt(jnp.mean(values * values, axis=-1, keepdims=True) + epsilon)
    return values * scale * gain


def merge_state(earlier, later):
    early_total, early_matrix, early_max = earlier
    late_total, late_matrix, late_max = later
    top_log = jnp.maximum(late_total + early_max, late_max)
    weight_early = jnp.exp(late_total + early_max - top_log)
    weight_late = jnp.exp(late_max - top_log)
    merged_matrix = (
        weight_early[:, None, None] * early_matrix + weight_late[:, None, None] * late_matrix
    )
    return (early_total + late_total, merged_matrix, top_log)


def block_summary(key_rows, value_rows, cumulative, in_gate):
    block_total = cumulative[-1]
    gap_logs = block_total[None, :] - cumulative + in_gate
    top_log = jnp.max(gap_logs, axis=0)
    weights = jnp.exp(gap_logs - top_log[None, :])
    part_matrix = jnp.einsum("sh,shd,she->hde", weights, key_rows, value_rows, precision=peak_value)
    return (block_total, part_matrix, top_log)


def memory_output(queries, key_rows, value_rows, cumulative, in_gate, state):
    _, state_matrix, state_max = state
    length = queries.shape[0]
    causal = jnp.tril(jnp.ones((length, length), dtype=bool))
    spread = cumulative[:, None, :] - cumulative[None, :, :] + in_gate[None, :, :]
    spread = jnp.where(causal[:, :, None], spread, floor_neg)
    carried_log = cumulative + state_max[None, :]
    running = jnp.maximum(carried_log, jnp.max(spread, axis=1))
    carried = jnp.exp(carried_log - running)
    scores = jnp.einsum("thd,shd->tsh", queries, key_rows, precision=peak_value) * jnp.exp(
        spread - running[:, None, :]
    )
    numerator = carried[:, :, None] * jnp.einsum(
        "thd,hde->the", queries, state_matrix, precision=peak_value
    )
    return numerator + jnp.einsum("tsh,she->the", scores, value_rows, precision=peak_value)


def memory_branch(
    normed,
    memory_query,
    memory_key,
    memory_value,
    memory_outgate,
    memory_ingate,
    memory_forget,
    forget_bias,
    forget_shift,
    memory_gain,
):
    tok_rows = normed.shape[0]
    proj_width = memory_query.shape[1]
    head_count = memory_ingate.shape[1]
    head_width = proj_width // head_count
    pieces = (
        lax.all_gather(memory_query, "fs", axis=0, tiled=True),
        lax.all_gather(memory_key, "fs", axis=0, tiled=True),
        lax.all_gather(memory_value, "fs", axis=0, tiled=True),
        lax.all_gather(memory_outgate, "fs", axis=0, tiled=True),
    )
    projected = tuple(
        (
            jnp.dot(normed, weight_piece, preferred_element_type=jnp.float32)
            for weight_piece in pieces
        )
    )
    segment_list = tok_rows // BLOCK
    block_shape = (segment_list, BLOCK, head_count, head_width)
    queries = rounded(projected[0]).reshape(block_shape)
    key_rows = (rounded(projected[1]) * head_width ** (-0.5)).reshape(block_shape)
    value_rows = rounded(projected[2]).reshape(block_shape)
    out_gate = jax.nn.sigmoid(rounded(projected[3])).reshape(tok_rows, head_count, head_width)
    in_gate = jnp.dot(normed, memory_ingate, preferred_element_type=jnp.float32).reshape(
        segment_list, BLOCK, head_count
    )
    log_forget = (
        jax.nn.log_sigmoid(
            jnp.dot(normed, memory_forget, preferred_element_type=jnp.float32) + forget_bias
        )
        + forget_shift[0]
    )
    cumulative = jnp.cumsum(log_forget.reshape(segment_list, BLOCK, head_count), axis=1)
    zero_heads = jnp.zeros((head_count,), jnp.float32)
    empty_memory_grid = jnp.zeros((head_count, head_width, head_width), jnp.float32)
    identity = (zero_heads, empty_memory_grid, jnp.full((head_count,), floor_neg, jnp.float32))
    prefixes = []
    running = identity
    for block_index in range(segment_list):
        prefixes.append(running)
        running = merge_state(
            running,
            block_summary(
                key_rows[block_index],
                value_rows[block_index],
                cumulative[block_index],
                in_gate[block_index],
            ),
        )
    dev_total, dev_matrix, dev_max = running
    incoming = carried_in((dev_total, dev_matrix, dev_max), "sp", merge_state, identity)
    outputs = []
    for block_index in range(segment_list):
        state = merge_state(incoming, prefixes[block_index])
        outputs.append(
            memory_output(
                queries[block_index],
                key_rows[block_index],
                value_rows[block_index],
                cumulative[block_index],
                in_gate[block_index],
                state,
            )
        )
    memory_out = jnp.concatenate(outputs, axis=0)
    mixed_heads = per_head_norm(out_gate * memory_out, memory_gain.reshape(head_count, head_width))
    return mixed_heads.reshape(tok_rows, proj_width).astype(jnp.bfloat16)


def fragment_summands(queries, kv_piece, head_bias, query_pos, key_start, strict):
    head_count, head_width = (queries.shape[1], queries.shape[2])
    key_count = kv_piece.shape[1]
    key_rows = kv_piece[0].reshape(key_count, head_count, head_width)
    value_rows = kv_piece[1].reshape(key_count, head_count, head_width)
    logits = jnp.einsum("thd,shd->hts", queries, key_rows, preferred_element_type=jnp.float32)
    logits = logits * head_width ** (-0.5) + head_bias[:, None, None]
    key_pos = key_start + jnp.arange(key_count, dtype=jnp.int32)
    visible = (key_pos[None, :] < query_pos[:, None]) & (key_pos[None, :] >= 0)
    keep_log = jnp.where(visible[None], jax.nn.log_sigmoid(-logits), jnp.float32(0.0))
    after = jnp.einsum("htj,js->hts", keep_log, strict, precision=peak_value)
    weights = jnp.where(
        visible[None], jnp.exp(jax.nn.log_sigmoid(logits) + after), jnp.float32(0.0)
    ).astype(jnp.bfloat16)
    part_out = jnp.einsum("hts,shd->thd", weights, value_rows, preferred_element_type=jnp.float32)
    return (part_out, jnp.sum(keep_log, axis=2).T)


def stick_branch(normed, stick_query, stick_key, stick_value, stick_bias, stick_gain):
    tok_rows = normed.shape[0]
    proj_width = stick_query.shape[1]
    head_count = stick_bias.shape[0]
    head_width = proj_width // head_count
    queries = (
        jnp.dot(normed, stick_query, preferred_element_type=jnp.float32)
        .astype(jnp.bfloat16)
        .reshape(tok_rows, head_count, head_width)
    )
    key_rows = jnp.dot(normed, stick_key, preferred_element_type=jnp.float32).astype(jnp.bfloat16)
    value_rows = jnp.dot(normed, stick_value, preferred_element_type=jnp.float32).astype(
        jnp.bfloat16
    )
    kv_pair = jnp.stack([key_rows, value_rows])
    sp_index = lax.axis_index("sp")
    sp_count = lax.axis_size("sp")
    positions = jnp.arange(tok_rows, dtype=jnp.int32)
    query_pos = sp_index * tok_rows + positions
    strict = (positions[:, None] > positions[None, :]).astype(jnp.float32)
    own_out, own_keep = fragment_summands(
        queries, kv_pair, stick_bias, query_pos, sp_index * tok_rows, strict
    )

    def turn(turn_index, state_carry):
        buffer, accumulated, running_sum = state_carry
        buffer = shifted(buffer, "sp", 1)
        source = sp_index - turn_index
        part_out, part_keep = fragment_summands(
            queries, buffer, stick_bias, query_pos, source * tok_rows, strict
        )
        return (
            buffer,
            accumulated + jnp.exp(running_sum)[:, :, None] * part_out,
            running_sum + part_keep,
        )

    _, stick_out, _ = lax.fori_loop(1, sp_count, turn, (kv_pair, own_out, own_keep))
    mixed_heads = per_head_norm(stick_out, stick_gain.reshape(head_count, head_width))
    return mixed_heads.reshape(tok_rows, proj_width).astype(jnp.bfloat16)


def per_device(
    tokens,
    norm_gain,
    memory_query,
    memory_key,
    memory_value,
    memory_outgate,
    memory_ingate,
    memory_forget,
    forget_bias,
    forget_shift,
    stick_query,
    stick_key,
    stick_value,
    stick_bias,
    memory_gain,
    stick_gain,
    out_memory,
    out_stick,
):
    gathered = lax.all_gather(tokens, "tp", axis=2, tiled=True)[0]
    values = gathered.astype(jnp.float32)
    normed = (
        values * lax.rsqrt(jnp.mean(values * values, axis=-1, keepdims=True) + epsilon) * norm_gain
    ).astype(jnp.bfloat16)
    mix_memory = memory_branch(
        normed,
        memory_query,
        memory_key,
        memory_value,
        memory_outgate,
        memory_ingate,
        memory_forget,
        forget_bias,
        forget_shift,
        memory_gain,
    )
    mix_stick = stick_branch(normed, stick_query, stick_key, stick_value, stick_bias, stick_gain)
    summed = lax.psum_scatter(
        (
            jnp.dot(mix_memory, out_memory, preferred_element_type=jnp.float32)
            + jnp.dot(mix_stick, out_stick, preferred_element_type=jnp.float32)
        ).astype(jnp.bfloat16),
        "tp",
        scatter_dimension=0,
        tiled=True,
    )
    return summed[None]


def solution(mesh):
    return jax.shard_map(
        per_device,
        mesh=mesh,
        in_specs=(
            P("fs", "sp", "tp"),
            P(),
            P("fs", "tp"),
            P("fs", "tp"),
            P("fs", "tp"),
            P("fs", "tp"),
            P(None, "tp"),
            P(None, "tp"),
            P("tp"),
            P("fs", "sp", "tp"),
            P(None, "tp"),
            P(None, "tp"),
            P(None, "tp"),
            P("tp"),
            P("tp"),
            P("tp"),
            P("tp", None),
            P("tp", None),
        ),
        out_specs=P("fs", ("sp", "tp"), None),
        check_vma=False,
    )
```

profile of v0, /device:TPU:0, one launch (start us, length us, event | category | flops | bytes accessed | tf_op | source)
XLA Modules:
  0.0 249.7 jit_solution(967684766303306881)
XLA Ops:
  10.8 9.9 %all-gather.10.cloned.1.call-done = bf16[1,256,2048]{2,1,0:T(8,128)(2,1)} async-done(((bf16[1,256,1024]{2,1,0:T(8,128)(2,1)}), bf16[1,256,2048]{2,1,0:T(8,128)(2,1)}) %all-gather.10.cloned.1.call-update) | async-done | bytes 1048592 | tf_op jit(solution)/shard_map/all_gather | solution.py:250
  20.7 1.6 fusion.24
  22.3 1.7 fusion.81
  26.2 1.9 convolution_convert_fusion.4
  28.1 1.4 convolution_convert_fusion.6
  29.9 1.9 fusion.33
  32.9 1.9 convolution_convert_fusion.5
  36.8 38.1 %while.33 = (s32[]{:T(128)}, bf16[2,256,256]{1,2,0:T(8,128)(2,1)S(1)}, f32[256,2,128]{2,0,1:T(8,128)S(1)}, f32[256,2]{0,1:T(2,128)}, s32[]{:T(128)}, /*index=5*/...) while((s32[]{:T(128)}, bf16[2,256,256]{1,2,0:T(8,128)(2,1)S(1)}, ...), condition=%wide.region_12.13_spmd.clone, body=%wide.region_10.12_spmd.clone.sunk | while | flops 475464704 | bytes 5538545 | solution.py:225
  36.8 3.8 %collective-permute-start = (bf16[2,256,256]{1,2,0:T(8,128)(2,1)S(1)}, bf16[2,256,256]{1,2,0:T(8,128)(2,1)S(1)}, u32[]{:S(2)}, u32[]{:S(2)}) collective-permute-start(bf16[2,256,256]{1,2,0:T(8,128)(2,1)S(1)} %get-tuple-element.490), channel_id=1, source_target_pairs={{0,8},{8,16},{16,24},{1,9},{9,17},{17,25},{2,10},{10,18},{18,26},{... | collective-permute-start | bytes 786440 | tf_op jit(solution)/shard_map/while/body/eval_jaxpr/ppermute | solution.py:39
  40.8 5.8 %collective-permute-done = bf16[2,256,256]{1,2,0:T(8,128)(2,1)S(1)} collective-permute-done((bf16[2,256,256]{1,2,0:T(8,128)(2,1)S(1)}, bf16[2,256,256]{1,2,0:T(8,128)(2,1)S(1)}, u32[]{:S(2)}, u32[]{:S(2)}) %collective-permute-start) | collective-permute-done | bytes 262176 | tf_op jit(solution)/shard_map/while/body/eval_jaxpr/ppermute | solution.py:39
  50.0 4.4 %collective-permute-start = (bf16[2,256,256]{1,2,0:T(8,128)(2,1)S(1)}, bf16[2,256,256]{1,2,0:T(8,128)(2,1)S(1)}, u32[]{:S(2)}, u32[]{:S(2)}) collective-permute-start(bf16[2,256,256]{1,2,0:T(8,128)(2,1)S(1)} %get-tuple-element.490), channel_id=1, source_target_pairs={{0,8},{8,16},{16,24},{1,9},{9,17},{17,25},{2,10},{10,18},{18,26},{... | collective-permute-start | bytes 786440 | tf_op jit(solution)/shard_map/while/body/eval_jaxpr/ppermute | solution.py:39
  54.5 4.9 %collective-permute-done = bf16[2,256,256]{1,2,0:T(8,128)(2,1)S(1)} collective-permute-done((bf16[2,256,256]{1,2,0:T(8,128)(2,1)S(1)}, bf16[2,256,256]{1,2,0:T(8,128)(2,1)S(1)}, u32[]{:S(2)}, u32[]{:S(2)}) %collective-permute-start) | collective-permute-done | bytes 262176 | tf_op jit(solution)/shard_map/while/body/eval_jaxpr/ppermute | solution.py:39
  62.8 4.4 %collective-permute-start = (bf16[2,256,256]{1,2,0:T(8,128)(2,1)S(1)}, bf16[2,256,256]{1,2,0:T(8,128)(2,1)S(1)}, u32[]{:S(2)}, u32[]{:S(2)}) collective-permute-start(bf16[2,256,256]{1,2,0:T(8,128)(2,1)S(1)} %get-tuple-element.490), channel_id=1, source_target_pairs={{0,8},{8,16},{16,24},{1,9},{9,17},{17,25},{2,10},{10,18},{18,26},{... | collective-permute-start | bytes 786440 | tf_op jit(solution)/shard_map/while/body/eval_jaxpr/ppermute | solution.py:39
  67.4 4.1 %collective-permute-done = bf16[2,256,256]{1,2,0:T(8,128)(2,1)S(1)} collective-permute-done((bf16[2,256,256]{1,2,0:T(8,128)(2,1)S(1)}, bf16[2,256,256]{1,2,0:T(8,128)(2,1)S(1)}, u32[]{:S(2)}, u32[]{:S(2)}) %collective-permute-start) | collective-permute-done | bytes 262176 | tf_op jit(solution)/shard_map/while/body/eval_jaxpr/ppermute | solution.py:39
  76.6 1.7 fusion.100
  82.4 2.3 convolution_convert_fusion.2
  85.0 10.9 %all-gather.16.cloned.1.call-done = bf16[2048,512]{1,0:T(8,128)(2,1)} async-done(((bf16[512,512]{1,0:T(8,128)(2,1)}), bf16[2048,512]{1,0:T(8,128)(2,1)}) %all-gather.16.cloned.1.call-update) | async-done | bytes 2097168 | tf_op jit(solution)/shard_map/all_gather | solution.py:109
  96.0 2.7 %convolution_convert_fusion.1 = bf16[256,512]{1,0:T(8,128)(2,1)S(1)} fusion(bf16[2048,512]{1,0:T(8,128)(2,1)} %all-gather.16.cloned.1.call-done, bf16[1,256,2048]{2,1,0:T(8,128)(2,1)} %all-gather.10.cloned.1.call-done, f32[2048]{0:T(1024)S(1)} %copy-done.39, f32[256]{0:T(256)S(1)} %copy-done.32), kind=kOutput, calls=%fused_computation.61 | convolution fusion | flops 539099136 | bytes 3417088 | tf_op jit(solution)/shard_map/dot_general | solution.py:114
  101.7 11.3 %all-gather.2 = bf16[4,1,2]{2,1,0:T(2,128)(2,1)} all-gather(bf16[1,1,2]{2,1,0:T(2,128)(2,1)} %fusion.85), channel_id=1, replica_groups=mesh['sp'=4,'fs'=4,'tp'=2] {'sp'}, dimensions={0}, use_global_device_ids=true | all-gather | bytes 20 | tf_op jit(solution)/shard_map/all_gather | solution.py:17
  113.0 9.0 %all-gather.1 = bf16[4,1,2]{2,1,0:T(2,128)(2,1)} all-gather(bf16[1,1,2]{2,1,0:T(2,128)(2,1)} %fusion.88), channel_id=1, replica_groups=mesh['sp'=4,'fs'=4,'tp'=2] {'sp'}, dimensions={0}, use_global_device_ids=true | all-gather | bytes 20 | tf_op jit(solution)/shard_map/all_gather | solution.py:17
  122.0 1.4 copy.88
  124.6 1.6 fusion.72
  126.2 3.0 %fusion.112 = f32[256,2048]{1,0:T(8,128)} fusion(bf16[256,256]{0,1:T(8,128)(2,1)S(1)} %bitcast.241, bf16[256,2048]{1,0:T(8,128)(2,1)} %param.39), kind=kOutput, calls=%fused_computation.186 | convolution fusion | flops 268435456 | bytes 3276800 | tf_op jit(solution)/shard_map/dot_general | solution.py:271
  129.3 3.6 %all-gather.18.cloned.1.call-done = bf16[2048,512]{1,0:T(8,128)(2,1)} async-done(((bf16[512,512]{1,0:T(8,128)(2,1)}), bf16[2048,512]{1,0:T(8,128)(2,1)}) %all-gather.18.cloned.1.call-update) | async-done | bytes 2097168 | tf_op jit(solution)/shard_map/all_gather | solution.py:107
  132.9 3.4 %convolution_convert_fusion = bf16[256,512]{1,0:T(8,128)(2,1)} fusion(bf16[2048,512]{1,0:T(8,128)(2,1)} %all-gather.18.cloned.1.call-done, bf16[1,256,2048]{2,1,0:T(8,128)(2,1)} %all-gather.10.cloned.1.call-done, f32[2048]{0:T(1024)} %param.23, f32[256]{0:T(256)} %copy-done.29), kind=kOutput, calls=%fused_computation.60 | convolution fusion | flops 539099136 | bytes 3417088 | tf_op jit(solution)/shard_map/dot_general | solution.py:114
  136.3 33.5 %all-gather.12.cloned.1.call-done = bf16[2048,512]{1,0:T(8,128)(2,1)} async-done(((bf16[512,512]{1,0:T(8,128)(2,1)}), bf16[2048,512]{1,0:T(8,128)(2,1)}) %all-gather.12.cloned.1.call-update) | async-done | bytes 2097168 | tf_op jit(solution)/shard_map/all_gather | solution.py:110
  169.8 2.7 %convolution_convert_fusion.3 = bf16[256,512]{1,0:T(8,128)(2,1)S(1)} fusion(bf16[2048,512]{1,0:T(8,128)(2,1)} %all-gather.12.cloned.1.call-done, bf16[1,256,2048]{2,1,0:T(8,128)(2,1)} %all-gather.10.cloned.1.call-done, f32[2048]{0:T(1024)S(1)} %copy-done.40, f32[256]{0:T(256)S(1)} %copy-done.33), kind=kOutput, calls=%fused_computation.63 | convolution fusion | flops 539099136 | bytes 3417088 | tf_op jit(solution)/shard_map/dot_general | solution.py:114
  174.3 1.7 fusion.109
  176.0 23.2 %all-gather.20.cloned.1.call-done = bf16[8,256,256]{2,1,0:T(8,128)(2,1)} async-done(((bf16[2,256,256]{2,1,0:T(8,128)(2,1)}), bf16[8,256,256]{2,1,0:T(8,128)(2,1)}) %all-gather.20.cloned.1.call-update) | async-done | bytes 1048592 | tf_op jit(solution)/shard_map/all_gather | solution.py:17
  205.3 1.4 fusion.38
  210.9 3.5 %fusion.23 = bf16[256,2048]{1,0:T(8,128)(2,1)} fusion(f32[256,2048]{1,0:T(8,128)} %fusion.112, bf16[512,2048]{1,0:T(8,128)(2,1)S(1)} %copy-done, f32[256,512]{1,0:T(8,128)S(1)} %bitcast.230, f32[128,512]{1,0:T(8,128)S(1)} %copy.136, f32[128,512]{1,0:T(8,128)} %copy.135, f32[512]{0:T(512)S(1)} %copy-done.26, bf16[256,512]{1,0:T(8,128)(2,1)S(1)} %copy-done.9), kind=kOutput, calls=%fused_computation.44 | convolution fusion | flops 539099136 | bytes 6555648 | tf_op jit(solution)/shard_map/dot_general | solution.py:270
  214.4 28.5 %reduce-scatter.2.cloned.1.call-done = bf16[128,2048]{1,0:T(8,128)(2,1)} async-done(((bf16[256,2048]{1,0:T(8,128)(2,1)}), bf16[128,2048]{1,0:T(8,128)(2,1)}) %reduce-scatter.2.cloned.1.call-update) | async-done | bytes 524304 | tf_op jit(solution)/shard_map/reduce_scatter | solution.py:268
  (200 shorter events, 42.3 us)
Async XLA Ops:
  6.5 204.3 %copy-start = (bf16[512,2048]{1,0:T(8,128)(2,1)S(1)}, bf16[512,2048]{1,0:T(8,128)(2,1)}, u32[]{:S(2)}) copy-start(bf16[512,2048]{1,0:T(8,128)(2,1)} %param.38) | copy-start | bytes 6291460
  6.5 15.8 %copy-start.36 = (f32[2048]{0:T(1024)S(1)}, f32[2048]{0:T(1024)}, u32[]{:S(2)}) copy-start(f32[2048]{0:T(1024)} %param.23) | copy-start | bytes 24580
  6.5 15.8 %copy-start.35 = (bf16[2048,2]{0,1:T(2,128)(2,1)S(1)}, bf16[2048,2]{0,1:T(2,128)(2,1)}, u32[]{:S(2)}) copy-start(bf16[2048,2]{0,1:T(2,128)(2,1)} %param.29) | copy-start | bytes 24580
  6.5 15.8 %copy-start.42 = (f32[2]{0:T(128)S(1)}, f32[2]{0:T(128)}, u32[]{:S(2)}) copy-start(f32[2]{0:T(128)} %param.30) | copy-start | bytes 28
  6.5 15.8 %copy-start.41 = (f32[1,256,2]{1,2,0:T(2,128)S(1)}, f32[1,256,2]{1,2,0:T(2,128)}, u32[]{:S(2)}) copy-start(f32[1,256,2]{1,2,0:T(2,128)} %param.31) | copy-start | bytes 6148
  6.5 14.1 %all-gather.10.cloned.1.call-start = ((), (), s32[]{:S(2)}) async-start(), calls=%async_computation.1 | async-start | bytes 1572864 | tf_op jit(solution)/shard_map/all_gather | solution.py:250
  7.3 75.1 %all-gather.14.cloned.1.call-start = ((), (), s32[]{:S(2)}) async-start(), calls=%async_computation.3 | async-start | bytes 2621440 | tf_op jit(solution)/shard_map/all_gather | solution.py:108
  8.0 87.9 %all-gather.16.cloned.1.call-start = ((), (), s32[]{:S(2)}) async-start(), calls=%async_computation.4 | async-start | bytes 2621440 | tf_op jit(solution)/shard_map/all_gather | solution.py:109
  8.8 124.1 %all-gather.18.cloned.1.call-start = ((), (), s32[]{:S(2)}) async-start(), calls=%async_computation.5 | async-start | bytes 2621440 | tf_op jit(solution)/shard_map/all_gather | solution.py:107
  9.3 160.4 %all-gather.12.cloned.1.call-start = ((), (), s32[]{:S(2)}) async-start(), calls=%async_computation.2 | async-start | bytes 2621440 | tf_op jit(solution)/shard_map/all_gather | solution.py:110
  9.9 189.3 %all-gather.20.cloned.1.call-start = ((), (), s32[]{:S(2)}) async-start(), calls=%async_computation.7 | async-start | bytes 1310720 | tf_op jit(solution)/shard_map/all_gather | solution.py:17
  20.7 5.5 %copy-start.10 = (bf16[1,256,2048]{2,1,0:T(8,128)(2,1)S(1)}, bf16[1,256,2048]{2,1,0:T(8,128)(2,1)}, u32[]{:S(2)}) copy-start(bf16[1,256,2048]{2,1,0:T(8,128)(2,1)} %all-gather.10.cloned.1.call-done) | copy-start | bytes 3145732
  36.8 39.7 %copy-start.18 = (f32[1,128,2]{2,1,0:T(8,128)S(1)}, f32[1,128,2]{2,1,0:T(8,128)}, u32[]{:S(2)}) copy-start(f32[1,128,2]{2,1,0:T(8,128)} %get-tuple-element.347) | copy-start | bytes 3076
  36.8 39.8 %copy-start.17 = (f32[1,128,2]{2,1,0:T(8,128)S(1)}, f32[1,128,2]{2,1,0:T(8,128)}, u32[]{:S(2)}) copy-start(f32[1,128,2]{2,1,0:T(8,128)} %get-tuple-element.346) | copy-start | bytes 3076
  36.8 9.8 %collective-permute-start = (bf16[2,256,256]{1,2,0:T(8,128)(2,1)S(1)}, bf16[2,256,256]{1,2,0:T(8,128)(2,1)S(1)}, u32[]{:S(2)}, u32[]{:S(2)}) collective-permute-start(bf16[2,256,256]{1,2,0:T(8,128)(2,1)S(1)} %get-tuple-element.490), channel_id=1, source_target_pairs={{0,8},{8,16},{16,24},{1,9},{9,17},{17,25},{2,10},{10,18},{18,26},{... | collective-permute-start | bytes 786440 | tf_op jit(solution)/shard_map/while/body/eval_jaxpr/ppermute | solution.py:39
  50.0 9.5 %collective-permute-start = (bf16[2,256,256]{1,2,0:T(8,128)(2,1)S(1)}, bf16[2,256,256]{1,2,0:T(8,128)(2,1)S(1)}, u32[]{:S(2)}, u32[]{:S(2)}) collective-permute-start(bf16[2,256,256]{1,2,0:T(8,128)(2,1)S(1)} %get-tuple-element.490), channel_id=1, source_target_pairs={{0,8},{8,16},{16,24},{1,9},{9,17},{17,25},{2,10},{10,18},{18,26},{... | collective-permute-start | bytes 786440 | tf_op jit(solution)/shard_map/while/body/eval_jaxpr/ppermute | solution.py:39
  62.8 8.7 %collective-permute-start = (bf16[2,256,256]{1,2,0:T(8,128)(2,1)S(1)}, bf16[2,256,256]{1,2,0:T(8,128)(2,1)S(1)}, u32[]{:S(2)}, u32[]{:S(2)}) collective-permute-start(bf16[2,256,256]{1,2,0:T(8,128)(2,1)S(1)} %get-tuple-element.490), channel_id=1, source_target_pairs={{0,8},{8,16},{16,24},{1,9},{9,17},{17,25},{2,10},{10,18},{18,26},{... | collective-permute-start | bytes 786440 | tf_op jit(solution)/shard_map/while/body/eval_jaxpr/ppermute | solution.py:39
  74.9 7.5 %copy-start.11 = (bf16[1,256,2048]{2,1,0:T(8,128)(2,1)S(1)}, bf16[1,256,2048]{2,1,0:T(8,128)(2,1)}, u32[]{:S(2)}) copy-start(bf16[1,256,2048]{2,1,0:T(8,128)(2,1)} %all-gather.10.cloned.1.call-done) | copy-start | bytes 3145732
  76.5 5.9 %copy-start.31 = (f32[256]{0:T(256)S(1)}, f32[256]{0:T(256)}, u32[]{:S(2)}) copy-start(f32[256]{0:T(256)} %copy-done.29) | copy-start | bytes 3076
  76.5 6.0 %copy-start.38 = (f32[2048]{0:T(1024)S(1)}, f32[2048]{0:T(1024)}, u32[]{:S(2)}) copy-start(f32[2048]{0:T(1024)} %param.23) | copy-start | bytes 24580
  76.5 8.2 %copy-start.22 = (f32[1,128,2]{1,2,0:T(2,128)}, f32[1,128,2]{1,2,0:T(2,128)S(1)}, u32[]{:S(2)}) copy-start(f32[1,128,2]{1,2,0:T(2,128)S(1)} %copy.140) | copy-start | bytes 3076
  76.6 8.1 %copy-start.21 = (f32[1,128,2]{1,2,0:T(2,128)}, f32[1,128,2]{1,2,0:T(2,128)S(1)}, u32[]{:S(2)}) copy-start(f32[1,128,2]{1,2,0:T(2,128)S(1)} %copy.141) | copy-start | bytes 3076
  84.8 11.2 %copy-start.32 = (f32[256]{0:T(256)S(1)}, f32[256]{0:T(256)}, u32[]{:S(2)}) copy-start(f32[256]{0:T(256)} %copy-done.29) | copy-start | bytes 3076
  84.8 11.2 %copy-start.39 = (f32[2048]{0:T(1024)S(1)}, f32[2048]{0:T(1024)}, u32[]{:S(2)}) copy-start(f32[2048]{0:T(1024)} %param.23) | copy-start | bytes 24580
  98.8 30.4 %copy-start.5 = (bf16[128,512]{0,1:T(8,128)(2,1)}, bf16[128,512]{0,1:T(8,128)(2,1)S(1)}, u32[]{:S(2)}) copy-start(bf16[128,512]{0,1:T(8,128)(2,1)S(1)} %copy.148) | copy-start | bytes 393220
  98.9 30.3 %copy-start.1 = (f32[128,512]{0,1:T(8,128)}, f32[128,512]{0,1:T(8,128)S(1)}, u32[]{:S(2)}) copy-start(f32[128,512]{0,1:T(8,128)S(1)} %copy.149) | copy-start | bytes 786436
  100.6 142.3 %reduce-scatter.2.cloned.1.call-start = ((), (), s32[]{:S(2)}) async-start(), calls=%async_computation.6 | async-start | bytes 1572864 | tf_op jit(solution)/shard_map/reduce_scatter | solution.py:268
  129.3 40.5 %copy-start.33 = (f32[256]{0:T(256)S(1)}, f32[256]{0:T(256)}, u32[]{:S(2)}) copy-start(f32[256]{0:T(256)} %copy-done.29) | copy-start | bytes 3076
  129.3 40.5 %copy-start.40 = (f32[2048]{0:T(1024)S(1)}, f32[2048]{0:T(1024)}, u32[]{:S(2)}) copy-start(f32[2048]{0:T(1024)} %param.23) | copy-start | bytes 24580
  199.8 7.2 %copy-start.6 = (bf16[128,512]{1,0:T(8,128)(2,1)S(1)}, bf16[128,512]{1,0:T(8,128)(2,1)}, u32[]{:S(2)}) copy-start(bf16[128,512]{1,0:T(8,128)(2,1)} %get-tuple-element.338) | copy-start | bytes 393220
  199.8 8.0 %copy-start.7 = (bf16[128,512]{1,0:T(8,128)(2,1)S(1)}, bf16[128,512]{1,0:T(8,128)(2,1)}, u32[]{:S(2)}) copy-start(bf16[128,512]{1,0:T(8,128)(2,1)} %get-tuple-element.339) | copy-start | bytes 393220
  203.8 5.4 %copy-start.4 = (f32[256,512]{0,1:T(8,128)S(1)}, f32[256,512]{0,1:T(8,128)}, u32[]{:S(2)}) copy-start(f32[256,512]{0,1:T(8,128)} %copy.137) | copy-start | bytes 1572868
  (25 other events, 49.2 us)
Sparse Core Ops, SparseCore 0:
  8.9 11.7 all-gather.9
  22.5 36.3 all-gather.13
  60.8 35.1 all-gather.15
  97.7 35.1 all-gather.17
  134.6 35.1 all-gather.11
  171.2 27.9 all-gather.19
  214.5 28.3 reduce-scatter.1
where the time goes:
time: 251 us; the launch traced here: 250 us
  waiting for transfers between devices  128 us (51%)
  matrix products  43.6 us (17%)
  blocking collectives  20.2 us (8%)
  other arithmetic  17.4 us (7%)
  between operations  14.1 us (6%)
  local copies, waits for them, and re-layouts  13.5 us (5%)
  starting transfers between devices  12.9 us (5%)
    all_gather x1, waiting for transfers between devices, memory_branch(): lax.all_gather(memory_outgate, 'fs', axis=0, tiled=True)  33.5 us
    reduce_scatter x1, waiting for transfers between devices, per_device(): lax.psum_scatter((jnp.dot(mix_memory, out_memory, preferred_element_type=...  28.5 us
    all_gather x1, waiting for transfers between devices, carried_in(): lax.all_gather(a.astype(kind), axis)  23.2 us
    all_gather x2, blocking collectives, carried_in(): lax.all_gather(a.astype(kind), axis)  20.2 us
    ppermute x3, waiting for transfers between devices, shifted(): return lax.ppermute(block, axis, route)  14.8 us
    ppermute x3, starting transfers between devices, shifted(): return lax.ppermute(block, axis, route)  12.6 us
    dot_general x4, matrix products, memory_branch(): jnp.dot(normed, weight_piece, preferred_element_type=jnp.float32)  11.1 us
    all_gather x1, waiting for transfers between devices, memory_branch(): lax.all_gather(memory_value, 'fs', axis=0, tiled=True)  10.9 us
  transfers between devices with their start and end apart: 10, of which 9 were waited for; matrix products, arithmetic and copies ran while one was open for 23% of the time, Pallas kernels for 0%

commit v1 on v0

v1 whole, which is shorter than its diff:
```python
import functools

import jax
import jax.numpy as jnp
from jax import lax
from jax.experimental import pallas as pl
from jax.experimental.pallas import tpu as pltpu
from jax.sharding import PartitionSpec as P

MESH = pl.DeviceIdType.MESH
epsilon = 1e-06
floor_neg = -1e30
f32 = jnp.float32
bf16 = jnp.bfloat16

KEY, VALUE, QUERY, GATE = 0, 1, 2, 3


def dot(a, b, dims=((1,), (0,))):
    return lax.dot_general(a, b, (dims, ((), ())), preferred_element_type=f32)


def softplus(z):
    return jnp.maximum(z, 0.0) + jnp.log(1.0 + jnp.exp(-jnp.abs(z)))


def kernel(
    n_sp,
    n_out,
    tok_ref,
    gain_ref,
    gatew_ref,
    bias_ref,
    shift_ref,
    sbias_ref,
    mgain_ref,
    sgain_ref,
    wk_hbm,
    wv_hbm,
    wq_hbm,
    wo_hbm,
    sq_hbm,
    sk_hbm,
    sv_hbm,
    om_hbm,
    os_hbm,
    out_ref,
    tok_in,
    nrm,
    xg,
    wm,
    ws,
    wout,
    sb1,
    rb1,
    sb2,
    rb2,
    proj,
    squery,
    kv,
    stick_acc,
    stick_run,
    gates,
    state_own,
    state_in,
    state_out,
    log_in,
    log_out,
    mix,
    ob,
    orb,
    load_sem,
    tok_s,
    tok_r,
    a2a_s,
    a2a_r,
    fwd_s,
    fwd_r,
    st1_s,
    st1_r,
    st2_s,
    st2_r,
    kv_s,
    kv_r,
    chain_s,
    chain_r,
    log_s,
    log_r,
    out_s,
    out_r,
):
    f = lax.axis_index("fs")
    s = lax.axis_index("sp")
    t = lax.axis_index("tp")
    rows, half_feat = tok_ref.shape
    heads = state_own.shape[0]
    dm = state_own.shape[1]
    ds = sgain_ref.shape[1] // heads
    block = wm.shape[1]
    half = rows // 2
    other = 1 - t

    def flip(bits):
        if bits == 3:
            return 3 - f
        if bits == 1:
            return f + 1 - 2 * (f % 2)
        return f + 2 - 4 * (f // 2)

    def remote(src, dst, send, recv, device):
        return pltpu.make_async_remote_copy(
            src_ref=src,
            dst_ref=dst,
            send_sem=send,
            recv_sem=recv,
            device_id=device,
            device_id_type=MESH,
        )

    width_s = ws.shape[2]
    loads = [
        pltpu.make_async_copy(sq_hbm, ws.at[0], load_sem.at[0]),
        pltpu.make_async_copy(sk_hbm, ws.at[1], load_sem.at[1]),
        pltpu.make_async_copy(sv_hbm, ws.at[2], load_sem.at[2]),
        pltpu.make_async_copy(wk_hbm, wm.at[0], load_sem.at[3]),
        pltpu.make_async_copy(wv_hbm, wm.at[1], load_sem.at[4]),
        pltpu.make_async_copy(wq_hbm, wm.at[2], load_sem.at[5]),
        pltpu.make_async_copy(wo_hbm, wm.at[3], load_sem.at[6]),
        pltpu.make_async_copy(om_hbm, wout.at[pl.ds(0, heads * dm)], load_sem.at[7]),
        pltpu.make_async_copy(os_hbm, wout.at[pl.ds(heads * dm, heads * ds)], load_sem.at[8]),
    ]
    for load in loads:
        load.start()

    barrier = pltpu.get_barrier_semaphore()
    pl.semaphore_signal(barrier, inc=1, device_id={"tp": other}, device_id_type=MESH)
    for bits in (1, 2, 3):
        pl.semaphore_signal(barrier, inc=1, device_id={"fs": flip(bits)}, device_id_type=MESH)

    @pl.when(s > 0)
    def _():
        pl.semaphore_signal(barrier, inc=1, device_id={"sp": s - 1}, device_id_type=MESH)

    @pl.when(s < n_sp - 1)
    def _():
        pl.semaphore_signal(barrier, inc=1, device_id={"sp": s + 1}, device_id_type=MESH)

    peers = 4 + jnp.where(s > 0, 1, 0) + jnp.where(s < n_sp - 1, 1, 0)
    pl.semaphore_wait(barrier, peers)

    tok_copy = remote(tok_ref, tok_in, tok_s.at[0], tok_r.at[0], {"tp": other})
    tok_copy.start()
    tok_copy.wait_recv()

    step_rows = 32
    own_cols = pl.ds(pl.multiple_of(t * half_feat, half_feat), half_feat)
    far_cols = pl.ds(pl.multiple_of(other * half_feat, half_feat), half_feat)

    def norm_rows(i, _):
        at = pl.ds(pl.multiple_of(i * step_rows, step_rows), step_rows)
        own = tok_ref[at, :].astype(f32)
        far = tok_in[at, :].astype(f32)
        total = jnp.sum(own * own, axis=1, keepdims=True) + jnp.sum(far * far, axis=1, keepdims=True)
        scale = lax.rsqrt(total / (2 * half_feat) + epsilon)
        nrm[at, own_cols] = (own * scale * gain_ref[:, own_cols]).astype(bf16)
        nrm[at, far_cols] = (far * scale * gain_ref[:, far_cols]).astype(bf16)
        return 0

    lax.fori_loop(0, rows // step_rows, norm_rows, 0)

    my_rows = pl.ds(pl.multiple_of(t * half, half), half)
    a2a, fwd = {}, {}
    for bits in (3, 1, 2):
        to = flip(bits)
        a2a[bits] = remote(
            nrm.at[my_rows, pl.ds(pl.multiple_of(to * block, block), block)],
            xg.at[bits, my_rows],
            a2a_s.at[bits - 1],
            a2a_r.at[bits - 1],
            {"fs": to},
        )
        a2a[bits].start()

    for load in loads[:3]:
        load.wait()
    normed = nrm[...]
    kv[0, 0] = dot(normed, ws[1]).astype(bf16)
    kv[0, 1] = dot(normed, ws[2]).astype(bf16)

    def kv_copy(d):
        return remote(kv.at[d - 1], kv.at[d], kv_s.at[d], kv_r.at[d], {"sp": s + 1})

    def kv_send(d):
        @pl.when((s < n_sp - 1) & (s >= d - 1))
        def _():
            kv_copy(d).start()

    kv_send(1)
    squery[...] = dot(normed, ws[0]).astype(bf16)
    xg[0] = nrm[:, pl.ds(pl.multiple_of(f * block, block), block)]

    for bits in (1, 2, 3):
        a2a[bits].wait_recv()
        fwd[bits] = remote(
            xg.at[bits, my_rows],
            xg.at[bits, my_rows],
            fwd_s.at[bits - 1],
            fwd_r.at[bits - 1],
            {"tp": other},
        )
        fwd[bits].start()
    for load in loads[3:]:
        load.wait()
    for bits in (1, 2, 3):
        fwd[bits].wait_recv()

    def order(h):
        return (1, 2) if h % 2 == 0 else (2, 1)

    def partial(p, h, seq):
        return dot(xg[seq], wm[p, :, h * dm : (h + 1) * dm])

    def first_copy(p, h, which):
        at = (p * heads + h) * 2 + which
        return remote(
            sb1.at[p, h, which], rb1.at[p, h, which], st1_s.at[at], st1_r.at[at],
            {"fs": flip(order(h)[0])},
        )

    def second_copy(p, h):
        at = p * heads + h
        return remote(
            sb2.at[p, h], rb2.at[p, h], st2_s.at[at], st2_r.at[at], {"fs": flip(order(h)[1])}
        )

    def first_step(p):
        for which, bits in ((1, 3), (0, None)):
            for h in range(heads):
                sb1[p, h, which] = partial(p, h, bits or order(h)[0]).astype(bf16)
                first_copy(p, h, which).start()

    def second_step(p):
        for h in range(heads):
            mine = partial(p, h, order(h)[1])
            first_copy(p, h, 1).wait_recv()
            sb2[p, h] = (mine + rb1[p, h, 1].astype(f32)).astype(bf16)
            second_copy(p, h).start()

    def finish(p, h):
        mine = partial(p, h, 0)
        first_copy(p, h, 0).wait_recv()
        second_copy(p, h).wait_recv()
        return (mine + rb1[p, h, 0].astype(f32) + rb2[p, h].astype(f32)).astype(bf16)

    for p in range(4):
        first_step(p)

    row_at = lax.broadcasted_iota(jnp.int32, (rows, rows), 0)
    col_at = lax.broadcasted_iota(jnp.int32, (rows, rows), 1)
    gate = dot(nrm[...], gatew_ref[...])
    log_forget = shift_ref[...] - softplus(-(gate + bias_ref[...]))
    tril = (row_at >= col_at).astype(f32)
    cumulative = lax.dot_general(
        tril, log_forget, (((1,), (0,)), ((), ())),
        precision=lax.Precision.HIGHEST, preferred_element_type=f32,
    )
    gates[0] = gate
    gates[1] = cumulative

    def stick_part(h, kv_at, diagonal):
        cols = slice(h * ds, (h + 1) * ds)
        z = dot(squery[:, cols], kv[kv_at, 0, :, cols], ((1,), (1,)))
        z = z * ds ** (-0.5) + sbias_ref[h]
        keep = -softplus(z)
        visible = col_at < row_at
        if diagonal:
            kept = jnp.where(visible, keep, 0.0)
        else:
            kept = keep
        strict = (row_at > col_at).astype(bf16)
        high = kept.astype(bf16)
        low = (kept - high.astype(f32)).astype(bf16)
        after = dot(high, strict) + dot(low, strict)
        weights = jnp.exp(z + keep + after)
        if diagonal:
            weights = jnp.where(visible, weights, 0.0)
        part = dot(weights.astype(bf16), kv[kv_at, 1, :, cols])
        return part, jnp.sum(kept, axis=1, keepdims=True)

    def stick_own():
        for h in range(heads):
            part, keep = stick_part(h, 0, True)
            stick_acc[h] = part
            stick_run[h] = jnp.broadcast_to(keep, stick_run.shape[1:])

    def stick_span(d):
        @pl.when(s >= d)
        def _():
            remote(kv.at[d - 1], kv.at[d], kv_s.at[d], kv_r.at[d], {"sp": s - 1}).wait_recv()

        kv_next(d)

        @pl.when(s >= d)
        def _():
            for h in range(heads):
                part, keep = stick_part(h, d, False)
                stick_acc[h] = stick_acc[h] + jnp.exp(stick_run[h]) * part
                stick_run[h] = stick_run[h] + keep

    def kv_next(d):
        @pl.when((s < n_sp - 1) & (s >= d) & (d < n_sp - 1))
        def _():
            kv_copy(d + 1).start()

    def stick_spans(low, high):
        if high > low:
            lax.fori_loop(low, high, lambda d, c: (stick_span(d), c)[1], 0)

    stick_own()
    second_step(KEY)
    stick_spans(1, min(2, n_sp))
    second_step(VALUE)

    def column(h):
        return gates[0, :, h : h + 1] - gates[1, :, heads + h : heads + h + 1]

    for h in range(heads):
        proj[KEY, h] = (finish(KEY, h).astype(f32) * dm ** (-0.5)).astype(bf16)
        proj[VALUE, h] = finish(VALUE, h)
        u = column(h)
        top = jnp.max(u, axis=0, keepdims=True)
        weighted = (proj[KEY, h].astype(f32) * jnp.exp(u - top)).astype(bf16)
        state_own[h] = dot(weighted, proj[VALUE, h], ((0,), (0,)))

    def log_copy(to):
        return remote(log_out, log_in, log_s.at[0], log_r.at[0], {"sp": to})

    def chain_copy(h, to):
        return remote(state_out.at[h], state_in.at[h], chain_s.at[h], chain_r.at[h], {"sp": to})

    def chain():
        @pl.when(s == 0)
        def _():
            log_in[...] = jnp.full(log_in.shape, floor_neg, f32)
            state_in[...] = jnp.zeros(state_in.shape, bf16)

        @pl.when(s > 0)
        def _():
            log_copy(s - 1).wait_recv()

        factors = []
        for h in range(heads):
            total = gates[1, rows - 1 : rows, heads + h : heads + h + 1]
            early = total + log_in[h : h + 1, 0:1]
            late = total + jnp.max(column(h), axis=0, keepdims=True)
            top = jnp.maximum(early, late)
            log_out[h : h + 1, :] = jnp.broadcast_to(top, (1, log_out.shape[1]))
            factors.append((jnp.exp(early - top), jnp.exp(late - top)))

        @pl.when(s < n_sp - 1)
        def _():
            log_copy(s + 1).start()

        for h in range(heads):

            @pl.when(s > 0)
            def _():
                chain_copy(h, s - 1).wait_recv()

            @pl.when(s < n_sp - 1)
            def _():
                early, late = factors[h]
                state_out[h] = (early * state_in[h].astype(f32) + late * state_own[h]).astype(bf16)
                chain_copy(h, s + 1).start()

    log_out[...] = jnp.zeros(log_out.shape, f32)
    pl.when(s == 0)(chain)
    second_step(QUERY)
    stick_spans(2, min(3, n_sp))
    pl.when(s == 1)(chain)
    second_step(GATE)
    stick_spans(3, n_sp)

    for h in range(heads):
        cols = slice(h * ds, (h + 1) * ds)
        out = stick_acc[h]
        scale = lax.rsqrt(jnp.mean(out * out, axis=1, keepdims=True) + epsilon)
        mix[:, heads * dm + h * ds : heads * dm + (h + 1) * ds] = (
            out * scale * sgain_ref[:, cols]
        ).astype(bf16)

    for h in range(heads):
        proj[QUERY, h] = finish(QUERY, h)
    pl.when(s > 1)(chain)

    gate_rows = jnp.transpose(gates[0] - pltpu.roll(gates[1], gates.shape[2] - heads, 1))
    causal = col_at <= row_at
    for h in range(heads):
        u_row = gate_rows[h : h + 1, :]
        carried_max = log_in[h : h + 1, 0:1]
        masked = jnp.where(causal, u_row, floor_neg)
        running = jnp.maximum(carried_max, jnp.max(masked, axis=1, keepdims=True))
        carried = jnp.exp(carried_max - running)
        queries = proj[QUERY, h]
        scores = dot(queries, proj[KEY, h], ((1,), (1,))) * jnp.exp(masked - running)
        memory = carried * dot(queries, state_in[h]) + dot(scores.astype(bf16), proj[VALUE, h])
        gated = memory / (1.0 + jnp.exp(-finish(GATE, h).astype(f32)))
        scale = lax.rsqrt(jnp.mean(gated * gated, axis=1, keepdims=True) + epsilon)
        cols = slice(h * dm, (h + 1) * dm)
        mix[:, cols] = (gated * scale * mgain_ref[:, cols]).astype(bf16)

    piece = wout.shape[1] // n_out
    far_rows = pl.ds(pl.multiple_of(other * half, half), half)
    copies = []
    for c in range(n_out):
        cols = slice(c * piece, (c + 1) * piece)
        ob[c] = dot(mix[far_rows, :], wout[:, cols]).astype(bf16)
        copy = remote(ob.at[c], orb.at[c], out_s.at[c], out_r.at[c], {"tp": other})
        copy.start()
        copies.append(copy)
    for c in range(n_out):
        cols = slice(c * piece, (c + 1) * piece)
        mine = dot(mix[my_rows, :], wout[:, cols])
        copies[c].wait_recv()
        out_ref[:, cols] = (mine + orb[c].astype(f32)).astype(bf16)

    tok_copy.wait_send()
    for bits in (1, 2, 3):
        a2a[bits].wait_send()
        fwd[bits].wait_send()
    for p in range(4):
        for h in range(heads):
            first_copy(p, h, 0).wait_send()
            first_copy(p, h, 1).wait_send()
            second_copy(p, h).wait_send()
    for copy in copies:
        copy.wait_send()

    @pl.when(s < n_sp - 1)
    def _():
        log_copy(s + 1).wait_send()
        for h in range(heads):
            chain_copy(h, s + 1).wait_send()

    def kv_done(d, c):
        @pl.when((s < n_sp - 1) & (s >= d - 1))
        def _():
            kv_copy(d).wait_send()

        return c

    if n_sp > 1:
        lax.fori_loop(1, n_sp, kv_done, 0)


def per_device(
    n_sp,
    tokens,
    norm_gain,
    memory_query,
    memory_key,
    memory_value,
    memory_outgate,
    memory_ingate,
    memory_forget,
    forget_bias,
    forget_shift,
    stick_query,
    stick_key,
    stick_value,
    stick_bias,
    memory_gain,
    stick_gain,
    out_memory,
    out_stick,
):
    rows, half_feat = tokens.shape[1:]
    features = 2 * half_feat
    heads = forget_bias.shape[0]
    block, width = memory_query.shape
    dm = width // heads
    stick_width = stick_query.shape[1]
    ds = stick_width // heads
    lanes = 128
    n_out = 4
    half = rows // 2

    gate_weight = jnp.pad(
        jnp.concatenate([memory_ingate, memory_forget], axis=1), ((0, 0), (0, lanes - 2 * heads))
    )
    bias = jnp.pad(forget_bias[None], ((0, 0), (heads, lanes - 2 * heads)))
    shift = jnp.pad(forget_shift[0], ((0, 0), (heads, lanes - 2 * heads)))

    vmem = pl.BlockSpec(memory_space=pltpu.VMEM)
    smem = pl.BlockSpec(memory_space=pltpu.SMEM)
    anyw = pl.BlockSpec(memory_space=pl.ANY)
    dma = pltpu.SemaphoreType.DMA
    out = pl.pallas_call(
        functools.partial(kernel, n_sp, n_out),
        out_shape=jax.ShapeDtypeStruct((half, features), bf16),
        in_specs=[vmem] * 5 + [smem] + [vmem] * 2 + [anyw] * 9,
        out_specs=vmem,
        scratch_shapes=[
            pltpu.VMEM((rows, half_feat), bf16),
            pltpu.VMEM((rows, features), bf16),
            pltpu.VMEM((4, rows, block), bf16),
            pltpu.VMEM((4, block, width), bf16),
            pltpu.VMEM((3, features, stick_width), bf16),
            pltpu.VMEM((width + stick_width, features), bf16),
            pltpu.VMEM((4, heads, 2, rows, dm), bf16),
            pltpu.VMEM((4, heads, 2, rows, dm), bf16),
            pltpu.VMEM((4, heads, rows, dm), bf16),
            pltpu.VMEM((4, heads, rows, dm), bf16),
            pltpu.VMEM((4, heads, rows, dm), bf16),
            pltpu.VMEM((rows, stick_width), bf16),
            pltpu.VMEM((n_sp, 2, rows, stick_width), bf16),
            pltpu.VMEM((heads, rows, ds), f32),
            pltpu.VMEM((heads, rows, ds), f32),
            pltpu.VMEM((2, rows, lanes), f32),
            pltpu.VMEM((heads, dm, dm), f32),
            pltpu.VMEM((heads, dm, dm), bf16),
            pltpu.VMEM((heads, dm, dm), bf16),
            pltpu.VMEM((8, lanes), f32),
            pltpu.VMEM((8, lanes), f32),
            pltpu.VMEM((rows, width + stick_width), bf16),
            pltpu.VMEM((n_out, half, features // n_out), bf16),
            pltpu.VMEM((n_out, half, features // n_out), bf16),
            dma((9,)),
            dma((1,)),
            dma((1,)),
            dma((3,)),
            dma((3,)),
            dma((3,)),
            dma((3,)),
            dma((8 * heads,)),
            dma((8 * heads,)),
            dma((4 * heads,)),
            dma((4 * heads,)),
            dma((n_sp,)),
            dma((n_sp,)),
            dma((heads,)),
            dma((heads,)),
            dma((1,)),
            dma((1,)),
            dma((n_out,)),
            dma((n_out,)),
        ],
        compiler_params=pltpu.CompilerParams(
            collective_id=0, has_side_effects=True, vmem_limit_bytes=60 * 1024 * 1024
        ),
    )(
        tokens[0],
        norm_gain[None],
        gate_weight,
        bias,
        shift,
        stick_bias,
        memory_gain[None],
        stick_gain[None],
        memory_key,
        memory_value,
        memory_query,
        memory_outgate,
        stick_query,
        stick_key,
        stick_value,
        out_memory,
        out_stick,
    )
    return out[None]


def solution(mesh):
    assert mesh.shape["fs"] == 4 and mesh.shape["tp"] == 2
    return jax.shard_map(
        functools.partial(per_device, mesh.shape["sp"]),
        mesh=mesh,
        in_specs=(
            P("fs", "sp", "tp"),
            P(),
            P("fs", "tp"),
            P("fs", "tp"),
            P("fs", "tp"),
            P("fs", "tp"),
            P(None, "tp"),
            P(None, "tp"),
            P("tp"),
            P("fs", "sp", "tp"),
            P(None, "tp"),
            P(None, "tp"),
            P(None, "tp"),
            P("tp"),
            P("tp"),
            P("tp"),
            P("tp", None),
            P("tp", None),
        ),
        out_specs=P("fs", ("sp", "tp"), None),
        check_vma=False,
    )
```

time: 251 us -> 76.4 us (0.30)
  the two profiles are of different devices: /device:TPU:0 before, /device:TPU:25 now
where the time goes in v1:
time: 76.4 us; the launch traced here: 76.1 us
  Pallas kernels  69.4 us (91%)
  local copies, waits for them, and re-layouts  5.92 us (8%)
    pallas_call x1, Pallas kernels, per_device(): pl.pallas_call(functools.partial(kernel, n_sp, n_out), out_shape=jax.Shap...  69.4 us
    unnamed x2, local copies, waits for them, and re-layouts  2.69 us

profile of v1, /device:TPU:25, one launch (start us, length us, event | category | flops | bytes accessed | tf_op | source)
XLA Modules:
  0.0 76.1 jit_solution(11046819871733505269)
XLA Ops:
  0.0 1.2 %pad.13.bias_ref = f32[1,128]{1,0:T(1,128)} pad(f32[1,2]{1,0:T(1,128)} %bitcast.13, f32[]{:T(128)} %constant.4.clone.1), padding=0_0x2_124 | pad | bytes 524 | tf_op jit(solution)/shard_map/jit(_pad)/pad | solution.py:491
  1.2 0.7 pad_maximum_fusion
  2.0 0.8 %copy.23 = f32[1,256,2]{2,1,0:T(8,128)S(1)} copy(f32[1,256,2]{1,2,0:T(2,128)} %param.27) | data formatting | bytes 4096 | tf_op args[9]
  2.8 0.8 %pad.14.shift_ref = f32[256,128]{1,0:T(8,128)} pad(f32[256,2]{1,0:T(8,128)S(1)} %bitcast.8, f32[]{:T(128)} %constant.4.clone.1), padding=0_0x2_124 | pad | bytes 133124 | tf_op jit(solution)/shard_map/jit(_pad)/pad | solution.py:492
  3.6 0.3 copy.22
  3.9 0.9 %pad.12.gatew_ref = bf16[2048,128]{1,0:T(8,128)(2,1)} pad(bf16[2048,4]{1,0:T(8,128)(2,1)S(1)} %copy.22, bf16[]{:T(256)} %constant.3.clone.1), padding=0_0x0_124 | pad | bytes 540674 | tf_op jit(solution)/shard_map/jit(_pad)/pad | solution.py:488
  4.8 69.4 %shard_map.172 = bf16[128,2048]{1,0:T(8,128)(2,1)} custom-call(bf16[256,1024]{1,0:T(8,128)(2,1)} %bitcast.9, f32[1,2048]{1,0:T(1,128)} %bitcast.10, bf16[2048,128]{1,0:T(8,128)(2,1)} %pad.12.gatew_ref, f32[1,128]{1,0:T(1,128)} %pad.13.bias_ref, f32[256,128]{1,0:T(8,128)} %pad.14.shift_ref, f32[2]{0:T(128)} %sbias_ref.1, f32[1,512]{1,0:T(1,128)} %bitcast.11, ...), custom_call_target="tpu_custom_call" | custom-call | tf_op jit(solution)/shard_map/pallas_call | solution.py:498
  74.2 1.9 %copy.25 = bf16[1,128,2048]{2,1,0:T(8,128)(2,1)} copy(bf16[1,128,2048]{2,1,0:T(8,128)(2,1)} %bitcast.7) | data formatting | bytes 1048576

commit v2 on v1

--- a/solution.py
+++ b/solution.py
@@ -29,7 +29,8 @@
     n_out,
     tok_ref,
     gain_ref,
-    gatew_ref,
+    ingate_ref,
+    forget_ref,
     bias_ref,
     shift_ref,
     sbias_ref,
@@ -49,18 +50,21 @@
     nrm,
     xg,
     wm,
+    wg,
     ws,
     wout,
-    sb1,
-    rb1,
-    sb2,
-    rb2,
+    sb,
+    rb,
+    own_part,
     proj,
     squery,
     kv,
     stick_acc,
     stick_run,
-    gates,
+    gw,
+    u_rows,
+    u_cols,
+    totals,
     state_own,
     state_in,
     state_out,
@@ -76,10 +80,10 @@
     a2a_r,
     fwd_s,
     fwd_r,
-    st1_s,
-    st1_r,
-    st2_s,
-    st2_r,
+    w_s,
+    w_r,
+    rs_s,
+    rs_r,
     kv_s,
     kv_r,
     chain_s,
@@ -150,6 +154,26 @@
 
     tok_copy = remote(tok_ref, tok_in, tok_s.at[0], tok_r.at[0], {"tp": other})
     tok_copy.start()
+
+    def pair_bits(h):
+        return 1 if h % 2 == 0 else 2
+
+    def sum_bits(h):
+        return 3 - pair_bits(h)
+
+    def weight_copy(p, h):
+        at = p * heads + h
+        return remote(
+            wm.at[p, :, pl.ds(h * dm, dm)], wg.at[p, h], w_s.at[at], w_r.at[at],
+            {"fs": flip(pair_bits(h))},
+        )
+
+    def send_weight(p):
+        loads[3 + p].wait()
+        for h in range(heads):
+            weight_copy(p, h).start()
+
+    send_weight(KEY)
     tok_copy.wait_recv()
 
     step_rows = 32
@@ -169,17 +193,24 @@
     lax.fori_loop(0, rows // step_rows, norm_rows, 0)
 
     my_rows = pl.ds(pl.multiple_of(t * half, half), half)
+
+    def feature_block(index):
+        return pl.ds(pl.multiple_of(index * block, block), block)
+
     a2a, fwd = {}, {}
-    for bits in (3, 1, 2):
-        to = flip(bits)
-        a2a[bits] = remote(
-            nrm.at[my_rows, pl.ds(pl.multiple_of(to * block, block), block)],
-            xg.at[bits, my_rows],
-            a2a_s.at[bits - 1],
-            a2a_r.at[bits - 1],
-            {"fs": to},
-        )
-        a2a[bits].start()
+    for h in range(heads):
+        for which in range(2):
+            at = h * 2 + which
+            to = flip(sum_bits(h))
+            a2a[at] = remote(
+                nrm.at[my_rows, feature_block(to if which == 0 else flip(3))],
+                xg.at[h, which, my_rows],
+                a2a_s.at[at],
+                a2a_r.at[at],
+                {"fs": to},
+            )
+            a2a[at].start()
+    send_weight(VALUE)
 
     for load in loads[:3]:
         load.wait()
@@ -197,75 +228,26 @@
 
     kv_send(1)
     squery[...] = dot(normed, ws[0]).astype(bf16)
-    xg[0] = nrm[:, pl.ds(pl.multiple_of(f * block, block), block)]
-
-    for bits in (1, 2, 3):
-        a2a[bits].wait_recv()
-        fwd[bits] = remote(
-            xg.at[bits, my_rows],
-            xg.at[bits, my_rows],
-            fwd_s.at[bits - 1],
-            fwd_r.at[bits - 1],
-            {"tp": other},
-        )
-        fwd[bits].start()
-    for load in loads[3:]:
-        load.wait()
-    for bits in (1, 2, 3):
-        fwd[bits].wait_recv()
-
-    def order(h):
-        return (1, 2) if h % 2 == 0 else (2, 1)
-
-    def partial(p, h, seq):
-        return dot(xg[seq], wm[p, :, h * dm : (h + 1) * dm])
-
-    def first_copy(p, h, which):
-        at = (p * heads + h) * 2 + which
-        return remote(
-            sb1.at[p, h, which], rb1.at[p, h, which], st1_s.at[at], st1_r.at[at],
-            {"fs": flip(order(h)[0])},
-        )
-
-    def second_copy(p, h):
-        at = p * heads + h
-        return remote(
-            sb2.at[p, h], rb2.at[p, h], st2_s.at[at], st2_r.at[at], {"fs": flip(order(h)[1])}
-        )
-
-    def first_step(p):
-        for which, bits in ((1, 3), (0, None)):
-            for h in range(heads):
-                sb1[p, h, which] = partial(p, h, bits or order(h)[0]).astype(bf16)
-                first_copy(p, h, which).start()
-
-    def second_step(p):
-        for h in range(heads):
-            mine = partial(p, h, order(h)[1])
-            first_copy(p, h, 1).wait_recv()
-            sb2[p, h] = (mine + rb1[p, h, 1].astype(f32)).astype(bf16)
-            second_copy(p, h).start()
-
-    def finish(p, h):
-        mine = partial(p, h, 0)
-        first_copy(p, h, 0).wait_recv()
-        second_copy(p, h).wait_recv()
-        return (mine + rb1[p, h, 0].astype(f32) + rb2[p, h].astype(f32)).astype(bf16)
-
-    for p in range(4):
-        first_step(p)
 
     row_at = lax.broadcasted_iota(jnp.int32, (rows, rows), 0)
     col_at = lax.broadcasted_iota(jnp.int32, (rows, rows), 1)
-    gate = dot(nrm[...], gatew_ref[...])
-    log_forget = shift_ref[...] - softplus(-(gate + bias_ref[...]))
-    tril = (row_at >= col_at).astype(f32)
-    cumulative = lax.dot_general(
-        tril, log_forget, (((1,), (0,)), ((), ())),
-        precision=lax.Precision.HIGHEST, preferred_element_type=f32,
-    )
-    gates[0] = gate
-    gates[1] = cumulative
+    gw[...] = jnp.zeros(gw.shape, bf16)
+    gw[0:heads, :] = ingate_ref[...]
+    gw[8 : 8 + heads, :] = forget_ref[...]
+    gate = dot(gw[...], normed, ((1,), (1,)))
+    triu = (row_at <= col_at).astype(f32)
+    u_rows[...] = jnp.zeros(u_rows.shape, f32)
+    for h in range(heads):
+        log_forget = shift_ref[h : h + 1, :] - softplus(-(gate[8 + h : 9 + h, :] + bias_ref[h]))
+        cumulative = lax.dot_general(
+            jnp.broadcast_to(log_forget, (8, rows)), triu, (((1,), (0,)), ((), ())),
+            precision=lax.Precision.HIGHEST, preferred_element_type=f32,
+        )
+        u_rows[h : h + 1, :] = gate[h : h + 1, :] - cumulative[0:1, :]
+        totals[h : h + 1, :] = jnp.broadcast_to(
+            cumulative[0:1, rows - 1 : rows], (1, totals.shape[1])
+        )
+    u_cols[...] = jnp.transpose(u_rows[...])
 
     def stick_part(h, kv_at, diagonal):
         cols = slice(h * ds, (h + 1) * ds)
@@ -317,12 +299,55 @@
             lax.fori_loop(low, high, lambda d, c: (stick_span(d), c)[1], 0)
 
     stick_own()
-    second_step(KEY)
+    for at in range(2 * heads):
+        a2a[at].wait_recv()
+        h, which = divmod(at, 2)
+        fwd[at] = remote(
+            xg.at[h, which, my_rows],
+            xg.at[h, which, my_rows],
+            fwd_s.at[at],
+            fwd_r.at[at],
+            {"tp": other},
+        )
+        fwd[at].start()
+
+    def rs_copy(p, h):
+        at = p * heads + h
+        return remote(
+            sb.at[p, h], rb.at[p, h], rs_s.at[at], rs_r.at[at], {"fs": flip(sum_bits(h))}
+        )
+
+    def partials(p):
+        for h in range(heads):
+            cols = slice(h * dm, (h + 1) * dm)
+            if p == KEY:
+                fwd[2 * h].wait_recv()
+                fwd[2 * h + 1].wait_recv()
+            weight_copy(p, h).wait_recv()
+            sb[p, h] = (dot(xg[h, 0], wm[p, :, cols]) + dot(xg[h, 1], wg[p, h])).astype(bf16)
+            rs_copy(p, h).start()
+
+    def own_partials(p):
+        for h in range(heads):
+            cols = slice(h * dm, (h + 1) * dm)
+            own_part[p, h] = dot(nrm[:, feature_block(f)], wm[p, :, cols]) + dot(
+                nrm[:, feature_block(flip(pair_bits(h)))], wg[p, h]
+            )
+
+    def finish(p, h):
+        rs_copy(p, h).wait_recv()
+        return (own_part[p, h] + rb[p, h].astype(f32)).astype(bf16)
+
+    partials(KEY)
+    own_partials(KEY)
+    partials(VALUE)
+    send_weight(QUERY)
+    send_weight(GATE)
+    own_partials(VALUE)
     stick_spans(1, min(2, n_sp))
-    second_step(VALUE)
 
     def column(h):
-        return gates[0, :, h : h + 1] - gates[1, :, heads + h : heads + h + 1]
+        return u_cols[:, h : h + 1]
 
     for h in range(heads):
         proj[KEY, h] = (finish(KEY, h).astype(f32) * dm ** (-0.5)).astype(bf16)
@@ -335,8 +360,15 @@
     def log_copy(to):
         return remote(log_out, log_in, log_s.at[0], log_r.at[0], {"sp": to})
 
-    def chain_copy(h, to):
-        return remote(state_out.at[h], state_in.at[h], chain_s.at[h], chain_r.at[h], {"sp": to})
+    piece_dm = dm // 2
+
+    def chain_copy(h, c, to):
+        cols = pl.ds(c * piece_dm, piece_dm)
+        at = h * 2 + c
+        return remote(
+            state_out.at[h, :, cols], state_in.at[h, :, cols], chain_s.at[at], chain_r.at[at],
+            {"sp": to},
+        )
 
     def chain():
         @pl.when(s == 0)
@@ -350,7 +382,7 @@
 
         factors = []
         for h in range(heads):
-            total = gates[1, rows - 1 : rows, heads + h : heads + h + 1]
+            total = totals[h : h + 1, 0:1]
             early = total + log_in[h : h + 1, 0:1]
             late = total + jnp.max(column(h), axis=0, keepdims=True)
             top = jnp.maximum(early, late)
@@ -361,25 +393,34 @@
         def _():
             log_copy(s + 1).start()
 
-        for h in range(heads):
+        for at in range(2 * heads):
+            h, c = divmod(at, 2)
+            cols = slice(c * piece_dm, (c + 1) * piece_dm)
 
             @pl.when(s > 0)
             def _():
-                chain_copy(h, s - 1).wait_recv()
+                chain_copy(h, c, s - 1).wait_recv()
 
             @pl.when(s < n_sp - 1)
             def _():
                 early, late = factors[h]
-                state_out[h] = (early * state_in[h].astype(f32) + late * state_own[h]).astype(bf16)
-                chain_copy(h, s + 1).start()
+                state_out[h, :, cols] = (
+                    early * state_in[h, :, cols].astype(f32) + late * state_own[h, :, cols]
+                ).astype(bf16)
+                chain_copy(h, c, s + 1).start()
 
     log_out[...] = jnp.zeros(log_out.shape, f32)
     pl.when(s == 0)(chain)
-    second_step(QUERY)
     stick_spans(2, min(3, n_sp))
+    partials(QUERY)
     pl.when(s == 1)(chain)
-    second_step(GATE)
+    own_partials(QUERY)
+    pl.when(s == 2)(chain)
+    partials(GATE)
+    own_partials(GATE)
     stick_spans(3, n_sp)
+    for load in loads[7:]:
+        load.wait()
 
     for h in range(heads):
         cols = slice(h * ds, (h + 1) * ds)
@@ -391,12 +432,11 @@
 
     for h in range(heads):
         proj[QUERY, h] = finish(QUERY, h)
-    pl.when(s > 1)(chain)
-
-    gate_rows = jnp.transpose(gates[0] - pltpu.roll(gates[1], gates.shape[2] - heads, 1))
+    pl.when(s > 2)(chain)
+
     causal = col_at <= row_at
     for h in range(heads):
-        u_row = gate_rows[h : h + 1, :]
+        u_row = u_rows[h : h + 1, :]
         carried_max = log_in[h : h + 1, 0:1]
         masked = jnp.where(causal, u_row, floor_neg)
         running = jnp.maximum(carried_max, jnp.max(masked, axis=1, keepdims=True))
@@ -425,22 +465,21 @@
         out_ref[:, cols] = (mine + orb[c].astype(f32)).astype(bf16)
 
     tok_copy.wait_send()
-    for bits in (1, 2, 3):
-        a2a[bits].wait_send()
-        fwd[bits].wait_send()
+    for at in range(2 * heads):
+        a2a[at].wait_send()
+        fwd[at].wait_send()
     for p in range(4):
         for h in range(heads):
-            first_copy(p, h, 0).wait_send()
-            first_copy(p, h, 1).wait_send()
-            second_copy(p, h).wait_send()
+            weight_copy(p, h).wait_send()
+            rs_copy(p, h).wait_send()
     for copy in copies:
         copy.wait_send()
 
     @pl.when(s < n_sp - 1)
     def _():
         log_copy(s + 1).wait_send()
-        for h in range(heads):
-            chain_copy(h, s + 1).wait_send()
+        for at in range(2 * heads):
+            chain_copy(at // 2, at % 2, s + 1).wait_send()
 
     def kv_done(d, c):
         @pl.when((s < n_sp - 1) & (s >= d - 1))
@@ -485,12 +524,6 @@
     n_out = 4
     half = rows // 2
 
-    gate_weight = jnp.pad(
-        jnp.concatenate([memory_ingate, memory_forget], axis=1), ((0, 0), (0, lanes - 2 * heads))
-    )
-    bias = jnp.pad(forget_bias[None], ((0, 0), (heads, lanes - 2 * heads)))
-    shift = jnp.pad(forget_shift[0], ((0, 0), (heads, lanes - 2 * heads)))
-
     vmem = pl.BlockSpec(memory_space=pltpu.VMEM)
     smem = pl.BlockSpec(memory_space=pltpu.SMEM)
     anyw = pl.BlockSpec(memory_space=pl.ANY)
@@ -498,25 +531,28 @@
     out = pl.pallas_call(
         functools.partial(kernel, n_sp, n_out),
         out_shape=jax.ShapeDtypeStruct((half, features), bf16),
-        in_specs=[vmem] * 5 + [smem] + [vmem] * 2 + [anyw] * 9,
+        in_specs=[vmem] * 4 + [smem, vmem, smem] + [vmem] * 2 + [anyw] * 9,
         out_specs=vmem,
         scratch_shapes=[
             pltpu.VMEM((rows, half_feat), bf16),
             pltpu.VMEM((rows, features), bf16),
-            pltpu.VMEM((4, rows, block), bf16),
+            pltpu.VMEM((heads, 2, rows, block), bf16),
             pltpu.VMEM((4, block, width), bf16),
+            pltpu.VMEM((4, heads, block, dm), bf16),
             pltpu.VMEM((3, features, stick_width), bf16),
             pltpu.VMEM((width + stick_width, features), bf16),
-            pltpu.VMEM((4, heads, 2, rows, dm), bf16),
-            pltpu.VMEM((4, heads, 2, rows, dm), bf16),
             pltpu.VMEM((4, heads, rows, dm), bf16),
             pltpu.VMEM((4, heads, rows, dm), bf16),
+            pltpu.VMEM((4, heads, rows, dm), f32),
             pltpu.VMEM((4, heads, rows, dm), bf16),
             pltpu.VMEM((rows, stick_width), bf16),
             pltpu.VMEM((n_sp, 2, rows, stick_width), bf16),
             pltpu.VMEM((heads, rows, ds), f32),
             pltpu.VMEM((heads, rows, ds), f32),
-            pltpu.VMEM((2, rows, lanes), f32),
+            pltpu.VMEM((16, features), bf16),
+            pltpu.VMEM((lanes, rows), f32),
+            pltpu.VMEM((rows, lanes), f32),
+            pltpu.VMEM((8, lanes), f32),
             pltpu.VMEM((heads, dm, dm), f32),
             pltpu.VMEM((heads, dm, dm), bf16),
             pltpu.VMEM((heads, dm, dm), bf16),
@@ -528,18 +564,18 @@
             dma((9,)),
             dma((1,)),
             dma((1,)),
-            dma((3,)),
-            dma((3,)),
-            dma((3,)),
-            dma((3,)),
-            dma((8 * heads,)),
-            dma((8 * heads,)),
+            dma((2 * heads,)),
+            dma((2 * heads,)),
+            dma((2 * heads,)),
+            dma((2 * heads,)),
+            dma((4 * heads,)),
+            dma((4 * heads,)),
             dma((4 * heads,)),
             dma((4 * heads,)),
             dma((n_sp,)),
             dma((n_sp,)),
-            dma((heads,)),
-            dma((heads,)),
+            dma((2 * heads,)),
+            dma((2 * heads,)),
             dma((1,)),
             dma((1,)),
             dma((n_out,)),
@@ -551,9 +587,10 @@
     )(
         tokens[0],
         norm_gain[None],
-        gate_weight,
-        bias,
-        shift,
+        memory_ingate.T,
+        memory_forget.T,
+        forget_bias,
+        forget_shift[0].T,
         stick_bias,
         memory_gain[None],
         stick_gain[None],

time: 76.4 us -> 52.8 us (0.69)
  the two profiles are of different devices: /device:TPU:25 before, /device:TPU:0 now
where the time goes in v2:
time: 52.8 us; the launch traced here: 52.6 us
  Pallas kernels  50.7 us (96%)
  local copies, waits for them, and re-layouts  1.88 us (4%)
    pallas_call x1, Pallas kernels, per_device(): pl.pallas_call(functools.partial(kernel, n_sp, n_out), out_shape=jax.Shap...  50.7 us
    unnamed x1, local copies, waits for them, and re-layouts  1.88 us

profile of v2, /device:TPU:0, one launch (start us, length us, event | category | flops | bytes accessed | tf_op | source)
XLA Modules:
  0.0 52.6 jit_solution(11878712041487737197)
XLA Ops:
  0.0 50.7 %shard_map.172 = bf16[128,2048]{1,0:T(8,128)(2,1)} custom-call(bf16[256,1024]{1,0:T(8,128)(2,1)} %bitcast.11, f32[1,2048]{1,0:T(1,128)} %bitcast.12, bf16[2,2048]{1,0:T(2,128)(2,1)} %bitcast.13, bf16[2,2048]{1,0:T(2,128)(2,1)} %bitcast.14, f32[2]{0:T(128)} %bias_ref.1, f32[2,256]{1,0:T(2,128)} %bitcast.15, f32[2]{0:T(128)} %sbias_ref.1, f32[1,512]{1,0:T(1,128)} %bitcast.16, ...), custom_call_target="tpu_custom_call" | custom-call | tf_op jit(solution)/shard_map/pallas_call | solution.py:531
  50.8 1.9 %copy.20 = bf16[1,128,2048]{2,1,0:T(8,128)(2,1)} copy(bf16[1,128,2048]{2,1,0:T(8,128)(2,1)} %bitcast.10) | data formatting | bytes 1048576

commit v3 on v2

--- a/solution.py
+++ b/solution.py
@@ -65,6 +65,7 @@
     u_rows,
     u_cols,
     totals,
+    tops,
     state_own,
     state_in,
     state_out,
@@ -121,6 +122,19 @@
             device_id_type=MESH,
         )
 
+    barrier = pltpu.get_barrier_semaphore()
+    pl.semaphore_signal(barrier, inc=1, device_id={"tp": other}, device_id_type=MESH)
+    for bits in (1, 2, 3):
+        pl.semaphore_signal(barrier, inc=1, device_id={"fs": flip(bits)}, device_id_type=MESH)
+
+    @pl.when(s > 0)
+    def _():
+        pl.semaphore_signal(barrier, inc=1, device_id={"sp": s - 1}, device_id_type=MESH)
+
+    @pl.when(s < n_sp - 1)
+    def _():
+        pl.semaphore_signal(barrier, inc=1, device_id={"sp": s + 1}, device_id_type=MESH)
+
     width_s = ws.shape[2]
     loads = [
         pltpu.make_async_copy(sq_hbm, ws.at[0], load_sem.at[0]),
@@ -133,21 +147,8 @@
         pltpu.make_async_copy(om_hbm, wout.at[pl.ds(0, heads * dm)], load_sem.at[7]),
         pltpu.make_async_copy(os_hbm, wout.at[pl.ds(heads * dm, heads * ds)], load_sem.at[8]),
     ]
-    for load in loads:
-        load.start()
-
-    barrier = pltpu.get_barrier_semaphore()
-    pl.semaphore_signal(barrier, inc=1, device_id={"tp": other}, device_id_type=MESH)
-    for bits in (1, 2, 3):
-        pl.semaphore_signal(barrier, inc=1, device_id={"fs": flip(bits)}, device_id_type=MESH)
-
-    @pl.when(s > 0)
-    def _():
-        pl.semaphore_signal(barrier, inc=1, device_id={"sp": s - 1}, device_id_type=MESH)
-
-    @pl.when(s < n_sp - 1)
-    def _():
-        pl.semaphore_signal(barrier, inc=1, device_id={"sp": s + 1}, device_id_type=MESH)
+    for at in (3, 4, 0, 1, 2, 5, 6, 7, 8):
+        loads[at].start()
 
     peers = 4 + jnp.where(s > 0, 1, 0) + jnp.where(s < n_sp - 1, 1, 0)
     pl.semaphore_wait(barrier, peers)
@@ -361,12 +362,14 @@
         return remote(log_out, log_in, log_s.at[0], log_r.at[0], {"sp": to})
 
     piece_dm = dm // 2
+    pieces = 4
 
     def chain_copy(h, c, to):
-        cols = pl.ds(c * piece_dm, piece_dm)
-        at = h * 2 + c
+        lines = pl.ds(c // 2 * piece_dm, piece_dm)
+        cols = pl.ds(c % 2 * piece_dm, piece_dm)
+        at = h * pieces + c
         return remote(
-            state_out.at[h, :, cols], state_in.at[h, :, cols], chain_s.at[at], chain_r.at[at],
+            state_out.at[h, lines, cols], state_in.at[h, lines, cols], chain_s.at[at], chain_r.at[at],
             {"sp": to},
         )
 
@@ -393,9 +396,10 @@
         def _():
             log_copy(s + 1).start()
 
-        for at in range(2 * heads):
-            h, c = divmod(at, 2)
-            cols = slice(c * piece_dm, (c + 1) * piece_dm)
+        for at in range(pieces * heads):
+            h, c = divmod(at, pieces)
+            lines = pl.ds(c // 2 * piece_dm, piece_dm)
+            cols = pl.ds(c % 2 * piece_dm, piece_dm)
 
             @pl.when(s > 0)
             def _():
@@ -404,8 +408,8 @@
             @pl.when(s < n_sp - 1)
             def _():
                 early, late = factors[h]
-                state_out[h, :, cols] = (
-                    early * state_in[h, :, cols].astype(f32) + late * state_own[h, :, cols]
+                state_out[h, lines, cols] = (
+                    early * state_in[h, lines, cols].astype(f32) + late * state_own[h, lines, cols]
                 ).astype(bf16)
                 chain_copy(h, c, s + 1).start()
 
@@ -430,21 +434,24 @@
             out * scale * sgain_ref[:, cols]
         ).astype(bf16)
 
+    causal = col_at <= row_at
     for h in range(heads):
         proj[QUERY, h] = finish(QUERY, h)
+        masked = jnp.where(causal, u_rows[h : h + 1, :], floor_neg)
+        top = jnp.max(masked, axis=1, keepdims=True)
+        scores = dot(proj[QUERY, h], proj[KEY, h], ((1,), (1,))) * jnp.exp(masked - top)
+        own_part[QUERY, h] = dot(scores.astype(bf16), proj[VALUE, h])
+        tops[h] = jnp.broadcast_to(top, tops.shape[1:])
     pl.when(s > 2)(chain)
-
-    causal = col_at <= row_at
     for h in range(heads):
-        u_row = u_rows[h : h + 1, :]
         carried_max = log_in[h : h + 1, 0:1]
-        masked = jnp.where(causal, u_row, floor_neg)
-        running = jnp.maximum(carried_max, jnp.max(masked, axis=1, keepdims=True))
-        carried = jnp.exp(carried_max - running)
-        queries = proj[QUERY, h]
-        scores = dot(queries, proj[KEY, h], ((1,), (1,))) * jnp.exp(masked - running)
-        memory = carried * dot(queries, state_in[h]) + dot(scores.astype(bf16), proj[VALUE, h])
-        gated = memory / (1.0 + jnp.exp(-finish(GATE, h).astype(f32)))
+        top = tops[h, :, 0:1]
+        running = jnp.maximum(carried_max, top)
+        own_part[QUERY, h] = jnp.exp(top - running) * own_part[QUERY, h] + jnp.exp(
+            carried_max - running
+        ) * dot(proj[QUERY, h], state_in[h])
+    for h in range(heads):
+        gated = own_part[QUERY, h] / (1.0 + jnp.exp(-finish(GATE, h).astype(f32)))
         scale = lax.rsqrt(jnp.mean(gated * gated, axis=1, keepdims=True) + epsilon)
         cols = slice(h * dm, (h + 1) * dm)
         mix[:, cols] = (gated * scale * mgain_ref[:, cols]).astype(bf16)
@@ -478,8 +485,8 @@
     @pl.when(s < n_sp - 1)
     def _():
         log_copy(s + 1).wait_send()
-        for at in range(2 * heads):
-            chain_copy(at // 2, at % 2, s + 1).wait_send()
+        for at in range(pieces * heads):
+            chain_copy(at // pieces, at % pieces, s + 1).wait_send()
 
     def kv_done(d, c):
         @pl.when((s < n_sp - 1) & (s >= d - 1))
@@ -530,7 +537,7 @@
     dma = pltpu.SemaphoreType.DMA
     out = pl.pallas_call(
         functools.partial(kernel, n_sp, n_out),
-        out_shape=jax.ShapeDtypeStruct((half, features), bf16),
+        out_shape=pltpu.VMEM((half, features), bf16),
         in_specs=[vmem] * 4 + [smem, vmem, smem] + [vmem] * 2 + [anyw] * 9,
         out_specs=vmem,
         scratch_shapes=[
@@ -553,6 +560,7 @@
             pltpu.VMEM((lanes, rows), f32),
             pltpu.VMEM((rows, lanes), f32),
             pltpu.VMEM((8, lanes), f32),
+            pltpu.VMEM((heads, rows, lanes), f32),
             pltpu.VMEM((heads, dm, dm), f32),
             pltpu.VMEM((heads, dm, dm), bf16),
             pltpu.VMEM((heads, dm, dm), bf16),
@@ -574,8 +582,8 @@
             dma((4 * heads,)),
             dma((n_sp,)),
             dma((n_sp,)),
-            dma((2 * heads,)),
-            dma((2 * heads,)),
+            dma((4 * heads,)),
+            dma((4 * heads,)),
             dma((1,)),
             dma((1,)),
             dma((n_out,)),

time: 52.8 us -> 50.3 us (0.953)
  Pallas kernels: 50.7 us -> 49.3 us
  local copies, waits for them, and re-layouts: 1.88 us -> 0.8 us
    pallas_call x1, Pallas kernels: 50.7 us -> 49.3 us  [per_device(): pl.pallas_call(functools.partial(kernel, n_sp, n_out), out_shape=pltpu.VM...]
    unnamed x1, local copies, waits for them, and re-layouts: 1.88 us -> 0.8 us
where the time goes in v3:
time: 50.3 us; the launch traced here: 50.1 us
  Pallas kernels  49.3 us (98%)
  local copies, waits for them, and re-layouts  0.8 us (2%)
    pallas_call x1, Pallas kernels, per_device(): pl.pallas_call(functools.partial(kernel, n_sp, n_out), out_shape=pltpu.VM...  49.3 us

profile of v3, /device:TPU:0, one launch (start us, length us, event | category | flops | bytes accessed | tf_op | source)
XLA Modules:
  0.0 50.1 jit_solution(1671164609220082631)
XLA Ops:
  0.0 49.3 %shard_map.172 = bf16[128,2048]{1,0:T(8,128)(2,1)S(1)} custom-call(bf16[256,1024]{1,0:T(8,128)(2,1)} %bitcast.11, f32[1,2048]{1,0:T(1,128)} %bitcast.12, bf16[2,2048]{1,0:T(2,128)(2,1)} %bitcast.13, bf16[2,2048]{1,0:T(2,128)(2,1)} %bitcast.14, f32[2]{0:T(128)} %bias_ref.1, f32[2,256]{1,0:T(2,128)} %bitcast.15, f32[2]{0:T(128)} %sbias_ref.1, ...), custom_call_target="tpu_custom_call" | custom-call | tf_op jit(solution)/shard_map/pallas_call | solution.py:538
  49.3 0.8 %copy.20 = bf16[1,128,2048]{2,1,0:T(8,128)(2,1)} copy(bf16[1,128,2048]{2,1,0:T(8,128)(2,1)S(1)} %bitcast.10) | data formatting | bytes 1048576
